TPU v7x, 32 devices: a whole 2x2x4 slice. The times are simulated.
32 devices in a mesh: sp: 8 (over z, x), tp: 4 (over y, core).
Axes of the slice: x: 2, y: 2, z: 4, core: 2. Of those that a mesh axis runs over, the one named last changes fastest.
Arguments:
- residual: bfloat16 [1024, 2048], P('sp'), may hold values from -6 to 6
- queries: bfloat16 [1024, 2048], P('sp', 'tp'), may hold values from -6 to 6
- keys: bfloat16 [1024, 2048], P('sp', 'tp'), may hold values from -6 to 6
- values: bfloat16 [1024, 2048], P('sp', 'tp'), may hold values from -24 to 24
- stick_bias: bfloat16 [32, 1024], P('tp', 'sp'), may hold values from 2 to 13
- query_gain: float32 [64], replicated, may hold values from 0.1 to 1.9
- key_gain: float32 [64], replicated, may hold values from 0.1 to 1.9
- out_weight: bfloat16 [2048, 2048], P('tp'), may hold values from -0.25 to 0.25
- norm_gain: float32 [2048], replicated, may hold values from 0.1 to 1.9
- route_ids: int32 [1024, 2], P('sp'), may hold values from 0 to 7, all different within a row; in each aligned block of 128 rows (0 to 127, 128 to 255, ...) at most 40 rows name the same one
- route_weights: float32 [1024, 2], P('sp'), may hold values from 0.1 to 1
- gate_weight: bfloat16 [8, 2048, 2048], P('sp', None, 'tp'), may hold values from -3 to 3
- up_weight: bfloat16 [8, 2048, 2048], P('sp', None, 'tp'), may hold values from -3 to 3
- down_weight: bfloat16 [8, 2048, 2048], P('sp', 'tp'), may hold values from -0.125 to 0.125
Outputs:
- layer_out: bfloat16 [1024, 2048], P('sp', 'tp')
Inputs may be any that keep to these rules, and one draw needn't show every extreme that they name: `route_ids`: each row names 2 different experts. In every aligned block of 128 rows at most 40 rows name one expert, and in every draw some expert is named by exactly 40 rows of some block.
All inputs are finite; a program needn't handle non-finite values.
Results may differ from a plain program's by a relative error of at most 0.028.
Values may be sent and summed in bfloat16 or wider, within the bound.
A program may use at most 64 MiB of HBM per device.

v0:
```python
import math
import jax
import jax.numpy as jnp
from jax import lax
from jax.sharding import PartitionSpec as P

epsilon = 1e-06
clamp_limit = 7.0
swish_scale = 1.702


def head_normalize(packed, gain):
    values_f = packed.astype(jnp.float32).reshape(packed.shape[0], -1, gain.shape[0])
    scaled = (
        values_f * lax.rsqrt(jnp.mean(values_f * values_f, axis=-1, keepdims=True) + epsilon) * gain
    )
    return scaled.astype(jnp.bfloat16)


def activate(gate_pre, up_pre):
    gate_top = jnp.minimum(gate_pre, clamp_limit)
    up_clip = jnp.clip(up_pre, -clamp_limit, clamp_limit)
    return (up_clip + 1.0) * (gate_top * jax.nn.sigmoid(swish_scale * gate_top))


def slot_table(picked, expert_count, capacity):
    flat_ids = picked.reshape(-1)
    one_hot = (flat_ids[:, None] == jnp.arange(expert_count, dtype=jnp.int32)[None, :]).astype(
        jnp.int32
    )
    before = jnp.sum((jnp.cumsum(one_hot, axis=0) - one_hot) * one_hot, axis=1)
    return flat_ids * capacity + before


def key_block(state_pair, queries_n, keys_block, values_block, bias_block, first_key, query_pos):
    summed, log_carry = state_pair
    key_count = bias_block.shape[1]
    head_total = bias_block.shape[0]
    keys_heads = keys_block.reshape(key_count, head_total, -1)
    values_heads = values_block.reshape(key_count, head_total, -1)
    head_dim = keys_heads.shape[2]
    scores = jnp.einsum(
        "qhd,khd->hqk", queries_n, keys_heads, preferred_element_type=jnp.float32
    ) * head_dim ** (-0.5)
    scores = scores - bias_block.astype(jnp.float32)[:, None, :]
    key_pos = first_key + jnp.arange(key_count, dtype=jnp.int32)
    causal = ((key_pos[None, :] < query_pos[:, None]) & (key_pos[None, :] >= 0))[None]
    log_stay = jnp.where(causal, jax.nn.log_sigmoid(-scores), 0.0)
    later_sum = lax.cumsum(log_stay, axis=2, reverse=True) - log_stay
    weight = jnp.where(
        causal, jnp.exp(jax.nn.log_sigmoid(scores) + later_sum + log_carry[:, :, None]), 0.0
    )
    summed = summed + jnp.einsum(
        "hqk,khd->qhd",
        weight.astype(jnp.bfloat16),
        values_heads,
        preferred_element_type=jnp.float32,
    )
    return (summed, log_carry + jnp.sum(log_stay, axis=2))


def per_device(
    residual,
    queries,
    keys,
    values,
    stick_bias,
    query_gain,
    key_gain,
    out_weight,
    norm_gain,
    route_ids,
    route_weights,
    gate_weight,
    up_weight,
    down_weight,
):
    tok_rows = queries.shape[0]
    width_sp = lax.axis_size("sp")
    offset = lax.axis_index("sp") * tok_rows
    query_pos = offset + jnp.arange(tok_rows, dtype=jnp.int32)
    queries_n = head_normalize(queries, query_gain)
    keys_n = head_normalize(keys, key_gain).reshape(tok_rows, -1)
    head_total = stick_bias.shape[0]
    head_dim = query_gain.shape[0]
    state_pair = (
        jnp.zeros((tok_rows, head_total, head_dim), jnp.float32),
        jnp.zeros((head_total, tok_rows), jnp.float32),
    )
    all_keys, all_values, all_bias = (
        lax.all_gather(keys_n, "sp", axis=0, tiled=True),
        lax.all_gather(values, "sp", axis=0, tiled=True),
        lax.all_gather(stick_bias, "sp", axis=1, tiled=True),
    )
    key_total = all_keys.shape[0]
    block_len = math.gcd(key_total, 512)
    block_total = key_total // block_len

    def sweep_block(block_step, running):
        first_key = (block_total - 1 - block_step) * block_len
        return key_block(
            running,
            queries_n,
            lax.dynamic_slice_in_dim(all_keys, first_key, block_len, 0),
            lax.dynamic_slice_in_dim(all_values, first_key, block_len, 0),
            lax.dynamic_slice_in_dim(all_bias, first_key, block_len, 1),
            first_key,
            query_pos,
        )

    state_pair = lax.fori_loop(0, block_total, sweep_block, state_pair)
    attended = state_pair[0].reshape(tok_rows, head_total * head_dim).astype(jnp.bfloat16)
    partial_value = jnp.dot(attended, out_weight, preferred_element_type=jnp.float32)
    model_width = residual.shape[1]
    expert_count = width_sp * gate_weight.shape[0]
    pick_count = route_ids.shape[1]
    capacity = (5 * tok_rows * pick_count + 4 * expert_count - 1) // (4 * expert_count)
    slot_index = slot_table(route_ids, expert_count, capacity)
    assigned = slot_index.shape[0]
    source = (
        jnp.zeros((expert_count * capacity,), jnp.int32)
        .at[slot_index]
        .set(jnp.arange(assigned, dtype=jnp.int32) // pick_count)
    )
    filled = (
        jnp.zeros((expert_count * capacity,), jnp.bfloat16)
        .at[slot_index]
        .set(jnp.ones((assigned,), jnp.bfloat16))
    )
    gate_local = gate_weight[0]
    up_local = up_weight[0]
    down_local = down_weight[0]
    mixed_share = lax.psum_scatter(
        partial_value.astype(jnp.bfloat16), "tp", scatter_dimension=1, tiled=True
    ).astype(jnp.float32)
    own_width = mixed_share.shape[1]
    col_start = lax.axis_index("tp") * own_width
    own_res = lax.dynamic_slice_in_dim(residual, col_start, own_width, 1).astype(jnp.float32)
    own_cols = (own_res + mixed_share).astype(jnp.bfloat16).astype(jnp.float32)
    square_total = lax.psum(jnp.sum(own_cols * own_cols, axis=1), "tp")
    gain_cols = lax.dynamic_slice_in_dim(norm_gain, col_start, own_width, 0)
    normed_share = (
        own_cols * lax.rsqrt(square_total / model_width + epsilon)[:, None] * gain_cols
    ).astype(jnp.bfloat16)
    outgoing = (normed_share[source] * filled[:, None]).reshape(expert_count, capacity, -1)
    piece = lax.all_gather(
        lax.all_to_all(outgoing, "sp", split_axis=0, concat_axis=0, tiled=True),
        "tp",
        axis=2,
        tiled=True,
    )
    gate_pre = jnp.einsum("scd,df->scf", piece, gate_local, preferred_element_type=jnp.float32)
    up_pre = jnp.einsum("scd,df->scf", piece, up_local, preferred_element_type=jnp.float32)
    hidden = activate(gate_pre, up_pre).astype(jnp.bfloat16)
    share = jnp.einsum("scf,fd->scd", hidden, down_local, preferred_element_type=jnp.float32)
    returned = lax.psum_scatter(share.astype(jnp.bfloat16), "tp", scatter_dimension=2, tiled=True)
    arrived = lax.all_to_all(returned, "sp", split_axis=0, concat_axis=0, tiled=True)
    columns = arrived.shape[2]
    taken_rows = arrived.reshape(expert_count * capacity, columns)[slot_index]
    taken_rows = taken_rows.astype(jnp.float32).reshape(tok_rows, pick_count, columns)
    routed = jnp.sum(taken_rows * route_weights[:, :, None], axis=1)
    return (own_cols + routed).astype(jnp.bfloat16)


def solution(mesh):
    placed = (
        P("sp", None),
        P("sp", "tp"),
        P("sp", "tp"),
        P("sp", "tp"),
        P("tp", "sp"),
        P(),
        P(),
        P("tp", None),
        P(),
        P("sp", None),
        P("sp", None),
        P("sp", None, "tp"),
        P("sp", None, "tp"),
        P("sp", "tp", None),
    )
    return jax.shard_map(
        per_device, mesh=mesh, in_specs=placed, out_specs=P("sp", "tp"), check_vma=False
    )
```

profile of v0, /device:TPU:0, one launch (start us, length us, event | category | flops | bytes accessed | tf_op | source)
XLA Modules:
  0.0 249.5 jit_solution(2540238676448930279)
XLA Ops:
  13.7 28.2 %all_gather.14 = bf16[8,1024]{1,0:T(8,128)(2,1)S(1)} all-gather(bf16[8,128]{1,0:T(8,128)(2,1)} %param.20), channel_id=1, replica_groups=mesh['sp'=8,'tp'=4] {'sp'}, dimensions={1}, use_global_device_ids=true | all-gather | bytes 18432 | tf_op jit(solution)/shard_map/all_gather | solution.py:93
  42.7 8.9 %all-gather.6.cloned.1.call-done = bf16[1024,512]{0,1:T(8,128)(2,1)} async-done(((bf16[128,512]{0,1:T(8,128)(2,1)}), bf16[1024,512]{0,1:T(8,128)(2,1)}) %all-gather.6.cloned.1.call-update) | async-done | bytes 1048592 | tf_op jit(solution)/shard_map/all_gather | solution.py:91
  51.6 40.3 %all-gather.4.cloned.1.call-done = bf16[1024,512]{0,1:T(8,128)(2,1)} async-done(((bf16[128,512]{0,1:T(8,128)(2,1)}), bf16[1024,512]{0,1:T(8,128)(2,1)}) %all-gather.4.cloned.1.call-update) | async-done | bytes 1048592 | tf_op jit(solution)/shard_map/all_gather | solution.py:92
  91.9 33.3 %while.16 = (s32[]{:T(128)}, f32[128,8,64]{0,2,1:T(8,128)S(1)}, f32[8,128]{1,0:T(8,128)S(1)}, bf16[1024,512]{0,1:T(8,128)(2,1)}, bf16[1024,512]{0,1:T(8,128)(2,1...) while((s32[]{:T(128)}, f32[128,8,64]{0,2,1:T(8,128)S(1)}, ...), condition=%wide.region_6.7_spmd.clone, body=%wide.region_2.6_spmd.clone.sunk | while | flops 219436672 | bytes 27240652 | solution.py:111
  93.4 3.0 %fusion.93 = (f32[8,128]{1,0:T(8,128)S(1)}, f32[8,128,512]{1,2,0:T(8,128)S(1)}, f32[8,512,128]{2,1,0:T(8,128)}) fusion(f32[8,512]{1,0:T(8,128)S(1)} %dynamic-slice_convert_fusion.2, pred[128,512]{0,1:T(8,128)(4,1)S(1)} %compare_and_fusion.2, bf16[512,8,64]{0,2,1:T(8,128)(2,1)S(1)} %bitcast.116, bf16[128,8,64]{0,2,1:T(8,128)(2,1)S(1)} %get-tuple-element.292), kind=kOutput, calls=%fused_computation.39.clone.1 | convolution fusion | flops 72875008 | bytes 4935680 | tf_op jit(solution)/shard_map/while/body/eval_jaxpr/qhd,khd->hqk/dot_general | solution.py:42
  96.4 5.0 %fusion.94 = f32[8,128,4,128]{1,0,3,2:T(8,128)S(1)} fusion(f32[8,128,4,128]{1,3,2,0:T(8,128)S(1)} %bitcast.114), kind=kOutput, calls=%fused_computation.23.clone.1 | output fusion | flops 66584576 | bytes 4194304 | tf_op jit(solution)/shard_map/reduce-window.6
  101.6 1.7 copy.38
  103.3 4.8 %fusion.97 = bf16[8,128,512]{1,2,0:T(8,128)(2,1)S(1)} fusion(f32[8,128,4,128]{1,3,2,0:T(8,128)} %copy.38, f32[8,512,128]{2,1,0:T(8,128)} %get-tuple-element.259, f32[8,128]{1,0:T(8,128)S(1)} %get-tuple-element.261, f32[8,512]{1,0:T(8,128)S(1)} %dynamic-slice_convert_fusion.2, pred[128,512]{0,1:T(8,128)(4,1)S(1)} %compare_and_fusion.2), kind=kLoop, calls=%fused_computation.12.clone.1 | loop fusion | flops 12058624 | bytes 5328896 | tf_op jit(solution)/shard_map/while/body/eval_jaxpr/convert_element_type | solution.py:55
  110.1 3.0 %fusion.93 = (f32[8,128]{1,0:T(8,128)S(1)}, f32[8,128,512]{1,2,0:T(8,128)S(1)}, f32[8,512,128]{2,1,0:T(8,128)}) fusion(f32[8,512]{1,0:T(8,128)S(1)} %dynamic-slice_convert_fusion.2, pred[128,512]{0,1:T(8,128)(4,1)S(1)} %compare_and_fusion.2, bf16[512,8,64]{0,2,1:T(8,128)(2,1)S(1)} %bitcast.116, bf16[128,8,64]{0,2,1:T(8,128)(2,1)S(1)} %get-tuple-element.292), kind=kOutput, calls=%fused_computation.39.clone.1 | convolution fusion | flops 72875008 | bytes 4935680 | tf_op jit(solution)/shard_map/while/body/eval_jaxpr/qhd,khd->hqk/dot_general | solution.py:42
  113.1 5.0 %fusion.94 = f32[8,128,4,128]{1,0,3,2:T(8,128)S(1)} fusion(f32[8,128,4,128]{1,3,2,0:T(8,128)S(1)} %bitcast.114), kind=kOutput, calls=%fused_computation.23.clone.1 | output fusion | flops 66584576 | bytes 4194304 | tf_op jit(solution)/shard_map/reduce-window.6
  118.3 1.7 copy.38
  120.0 4.8 %fusion.97 = bf16[8,128,512]{1,2,0:T(8,128)(2,1)S(1)} fusion(f32[8,128,4,128]{1,3,2,0:T(8,128)} %copy.38, f32[8,512,128]{2,1,0:T(8,128)} %get-tuple-element.259, f32[8,128]{1,0:T(8,128)S(1)} %get-tuple-element.261, f32[8,512]{1,0:T(8,128)S(1)} %dynamic-slice_convert_fusion.2, pred[128,512]{0,1:T(8,128)(4,1)S(1)} %compare_and_fusion.2), kind=kLoop, calls=%fused_computation.12.clone.1 | loop fusion | flops 12058624 | bytes 5328896 | tf_op jit(solution)/shard_map/while/body/eval_jaxpr/convert_element_type | solution.py:55
  125.2 2.9 %convolution_convert_fusion.1 = bf16[128,2048]{1,0:T(8,128)(2,1)} fusion(bf16[128,512]{0,1:T(8,128)(2,1)S(1)} %bitcast.118, bf16[512,2048]{1,0:T(8,128)(2,1)} %param.23), kind=kOutput, calls=%fused_computation.41 | convolution fusion | flops 268697600 | bytes 2752512 | tf_op jit(solution)/shard_map/dot_general | solution.py:113
  130.3 2.2 scatter_custom_fusion.1
  133.3 15.6 %reduce-scatter.3.cloned.1.call-done = bf16[128,512]{1,0:T(8,128)(2,1)} async-done(((bf16[128,2048]{1,0:T(8,128)(2,1)}), bf16[128,512]{1,0:T(8,128)(2,1)}) %reduce-scatter.3.cloned.1.call-update) | async-done | bytes 131088 | tf_op jit(solution)/shard_map/reduce_scatter | solution.py:133
  150.0 5.8 %psum.7 = f32[128]{0:T(128)S(1)} all-reduce(f32[128]{0:T(128)S(1)} %get-tuple-element.193), channel_id=1, replica_groups=mesh['sp'=8,'tp'=4] {'tp'}, use_global_device_ids=true, to_apply=%region_9.10 | all-reduce | flops 128 | bytes 1024 | tf_op jit(solution)/shard_map/psum | solution.py:140
  155.9 2.0 gather_fusion
  158.0 16.3 %all_to_all.10 = bf16[8,40,512]{2,1,0:T(8,128)(2,1)} all-to-all(bf16[8,40,512]{2,1,0:T(8,128)(2,1)S(1)} %broadcast_multiply_fusion), channel_id=1, replica_groups=mesh['sp'=8,'tp'=4] {'sp'}, dimensions={0} | all-to-all | bytes 655360 | tf_op jit(solution)/shard_map/all_to_all | solution.py:147
  174.6 15.6 %all-gather.8.cloned.1.call-done = bf16[8,40,2048]{2,1,0:T(8,128)(2,1)} async-done(((bf16[8,40,512]{2,1,0:T(8,128)(2,1)}), bf16[8,40,2048]{2,1,0:T(8,128)(2,1)}) %all-gather.8.cloned.1.call-update) | async-done | bytes 1310736 | tf_op jit(solution)/shard_map/all_gather | solution.py:146
  190.1 2.8 %fusion.33 = f32[8,40,512]{2,1,0:T(8,128)S(1)} fusion(bf16[8,40,2048]{2,1,0:T(8,128)(2,1)} %all-gather.8.cloned.1.call-done, bf16[1,2048,512]{2,1,0:T(8,128)(2,1)} %param.27), kind=kOutput, calls=%fused_computation.50 | convolution fusion | flops 671252480 | bytes 4063232 | tf_op jit(solution)/shard_map/scd,df->scf/dot_general | solution.py:152
  193.0 4.8 %convolution_convert_fusion = bf16[8,40,2048]{2,1,0:T(8,128)(2,1)} fusion(bf16[1,512,2048]{2,1,0:T(8,128)(2,1)S(1)} %copy-done, bf16[8,40,2048]{2,1,0:T(8,128)(2,1)} %all-gather.8.cloned.1.call-done, bf16[1,2048,512]{2,1,0:T(8,128)(2,1)} %param.28, f32[8,40,512]{2,1,0:T(8,128)S(1)} %fusion.33), kind=kOutput, calls=%fused_computation.40 | convolution fusion | flops 1344307200 | bytes 7471104 | tf_op jit(solution)/shard_map/scf,fd->scd/dot_general | solution.py:155
  197.8 26.6 %reduce-scatter.5.cloned.1.call-done = bf16[8,40,512]{2,1,0:T(8,128)(2,1)} async-done(((bf16[8,40,2048]{2,1,0:T(8,128)(2,1)}), bf16[8,40,512]{2,1,0:T(8,128)(2,1)}) %reduce-scatter.5.cloned.1.call-update) | async-done | bytes 327696 | tf_op jit(solution)/shard_map/reduce_scatter | solution.py:156
  224.4 5.5 %all-to-all-start.1 = ((bf16[8,40,512]{2,1,0:T(8,128)(2,1)}), bf16[8,40,512]{2,1,0:T(8,128)(2,1)S(1)}, u32[]{:S(2)}, u32[]{:S(2)}) async-start(bf16[8,40,512]{2,1,0:T(8,128)(2,1)} %reduce-scatter.5.cloned.1.call-done), calls=%async_computation.3 | async-start | bytes 655360 | tf_op jit(solution)/shard_map/all_to_all | solution.py:157
  230.0 10.0 %all-to-all-done.1 = bf16[8,40,512]{2,1,0:T(8,128)(2,1)S(1)} async-done(((bf16[8,40,512]{2,1,0:T(8,128)(2,1)}), bf16[8,40,512]{2,1,0:T(8,128)(2,1)S(1)}, u32[]{:S(2)}, u32[]{:S(2)}) %all-to-all-start.1) | async-done | bytes 327712 | tf_op jit(solution)/shard_map/all_to_all | solution.py:157
  (82 shorter events, 19.5 us)
Async XLA Ops:
  6.5 186.5 %copy-start = (bf16[1,512,2048]{2,1,0:T(8,128)(2,1)S(1)}, bf16[1,512,2048]{2,1,0:T(8,128)(2,1)}, u32[]{:S(2)}) copy-start(bf16[1,512,2048]{2,1,0:T(8,128)(2,1)} %param.29) | copy-start | bytes 6291460
  6.5 45.1 %all-gather.6.cloned.1.call-start = ((), (), s32[]{:S(2)}) async-start(), calls=%async_computation.5 | async-start | bytes 1179648 | tf_op jit(solution)/shard_map/all_gather | solution.py:91
  9.3 82.6 %all-gather.4.cloned.1.call-start = ((), (), s32[]{:S(2)}) async-start(), calls=%async_computation.4 | async-start | bytes 1179648 | tf_op jit(solution)/shard_map/all_gather | solution.py:92
  11.1 137.9 %reduce-scatter.3.cloned.1.call-start = ((), (), s32[]{:S(2)}) async-start(), calls=%async_computation.6 | async-start | bytes 655360 | tf_op jit(solution)/shard_map/reduce_scatter | solution.py:133
  125.1 3.4 %copy-start.1 = (s32[128,2]{0,1:T(2,128)S(1)}, s32[128,2]{0,1:T(2,128)}, u32[]{:S(2)}) copy-start(s32[128,2]{0,1:T(2,128)} %param.25) | copy-start | bytes 3076
  128.1 62.1 %all-gather.8.cloned.1.call-start = ((), (), s32[]{:S(2)}) async-start(), calls=%async_computation.7 | async-start | bytes 1638400 | tf_op jit(solution)/shard_map/all_gather | solution.py:146
  174.4 50.0 %reduce-scatter.5.cloned.1.call-start = ((), (), s32[]{:S(2)}) async-start(), calls=%async_computation.8 | async-start | bytes 1638400 | tf_op jit(solution)/shard_map/reduce_scatter | solution.py:156
  193.0 36.9 %copy-start.2 = (f32[128,2]{0,1:T(2,128)S(1)}, f32[128,2]{0,1:T(2,128)}, u32[]{:S(2)}) copy-start(f32[128,2]{0,1:T(2,128)} %param.26) | copy-start | bytes 3076
  224.4 15.7 %all-to-all-start.1 = ((bf16[8,40,512]{2,1,0:T(8,128)(2,1)}), bf16[8,40,512]{2,1,0:T(8,128)(2,1)S(1)}, u32[]{:S(2)}, u32[]{:S(2)}) async-start(bf16[8,40,512]{2,1,0:T(8,128)(2,1)} %reduce-scatter.5.cloned.1.call-done), calls=%async_computation.3 | async-start | bytes 655360 | tf_op jit(solution)/shard_map/all_to_all | solution.py:157
Sparse Core Ops, SparseCore 0:
  9.4 42.1 all-gather.5
  53.6 38.1 all-gather.3
  128.2 20.6 reduce-scatter.2
  174.5 15.6 all-gather.7
  197.9 26.4 reduce-scatter.4
where the time goes:
time: 250 us; the launch traced here: 249 us
  waiting for transfers between devices  117 us (47%)
  blocking collectives  50.3 us (20%)
  other arithmetic  25.5 us (10%)
  local copies, waits for them, and re-layouts  20.1 us (8%)
  matrix products  17.2 us (7%)
  between operations  13.4 us (5%)
  starting transfers between devices  5.86 us (2%)
    all_gather x1, waiting for transfers between devices, per_device(): lax.all_gather(values, 'sp', axis=0, tiled=True)  40.3 us
    all_gather x1, blocking collectives, per_device(): lax.all_gather(stick_bias, 'sp', axis=1, tiled=True)  28.2 us
    reduce_scatter x1, waiting for transfers between devices, per_device(): lax.psum_scatter(share.astype(jnp.bfloat16), 'tp', scatter_dimension=2, t...  26.6 us
    all_to_all x1, blocking collectives, per_device(): lax.all_to_all(outgoing, 'sp', split_axis=0, concat_axis=0, tiled=True)  16.3 us
    reduce_scatter x1, waiting for transfers between devices, per_device(): lax.psum_scatter(partial_value.astype(jnp.bfloat16), 'tp', scatter_dimens...  15.6 us
    all_gather x1, waiting for transfers between devices, per_device(): lax.all_gather(lax.all_to_all(outgoing, 'sp', split_axis=0, concat_axis=0...  15.6 us
    another operation x6, other arithmetic  10.7 us
    all_to_all x1, waiting for transfers between devices, per_device(): lax.all_to_all(returned, 'sp', split_axis=0, concat_axis=0, tiled=True)  10 us
  transfers between devices with their start and end apart: 6, of which 6 were waited for; matrix products, arithmetic and copies ran while one was open for 4% of the time, Pallas kernels for 0%

commit v1 on v0

--- a/solution.py
+++ b/solution.py
@@ -90,7 +90,7 @@
     all_keys, all_values, all_bias = (
         lax.all_gather(keys_n, "sp", axis=0, tiled=True),
         lax.all_gather(values, "sp", axis=0, tiled=True),
-        lax.all_gather(stick_bias, "sp", axis=1, tiled=True),
+        jnp.concatenate(lax.all_gather(stick_bias, "sp"), axis=1),
     )
     key_total = all_keys.shape[0]
     block_len = math.gcd(key_total, 512)

time: 250 us -> 250 us (level)
  no operation moved by 1% of the time
where the time goes in v1:
time: 250 us; the launch traced here: 249 us
  waiting for transfers between devices  117 us (47%)
  blocking collectives  50.3 us (20%)
  other arithmetic  25.5 us (10%)
  local copies, waits for them, and re-layouts  20.1 us (8%)
  matrix products  17.2 us (7%)
  between operations  13.4 us (5%)
  starting transfers between devices  5.86 us (2%)
    all_gather x1, waiting for transfers between devices, per_device(): lax.all_gather(values, 'sp', axis=0, tiled=True)  40.3 us
    all_gather x1, blocking collectives, per_device(): lax.all_gather(stick_bias, 'sp')  28.2 us
    reduce_scatter x1, waiting for transfers between devices, per_device(): lax.psum_scatter(share.astype(jnp.bfloat16), 'tp', scatter_dimension=2, t...  26.6 us
    all_to_all x1, blocking collectives, per_device(): lax.all_to_all(outgoing, 'sp', split_axis=0, concat_axis=0, tiled=True)  16.3 us
    reduce_scatter x1, waiting for transfers between devices, per_device(): lax.psum_scatter(partial_value.astype(jnp.bfloat16), 'tp', scatter_dimens...  15.6 us
    all_gather x1, waiting for transfers between devices, per_device(): lax.all_gather(lax.all_to_all(outgoing, 'sp', split_axis=0, concat_axis=0...  15.6 us
    another operation x6, other arithmetic  10.7 us
    all_to_all x1, waiting for transfers between devices, per_device(): lax.all_to_all(returned, 'sp', split_axis=0, concat_axis=0, tiled=True)  10 us
  transfers between devices with their start and end apart: 6, of which 6 were waited for; matrix products, arithmetic and copies ran while one was open for 4% of the time, Pallas kernels for 0%

profile of v1, /device:TPU:0, one launch (start us, length us, event | category | flops | bytes accessed | tf_op | source)
XLA Modules:
  0.0 249.5 jit_solution(15424628666111324970)
XLA Ops:
  13.7 28.2 %all-gather = bf16[64,128]{1,0:T(8,128)(2,1)S(1)} all-gather(bf16[8,128]{1,0:T(8,128)(2,1)} %param.20), channel_id=2, replica_groups=mesh['sp'=8,'tp'=4] {'sp'}, dimensions={0}, use_global_device_ids=true | all-gather | bytes 18432 | tf_op jit(solution)/shard_map/all_gather | solution.py:93
  42.7 8.9 %all-gather.7.cloned.1.call-done = bf16[1024,512]{0,1:T(8,128)(2,1)} async-done(((bf16[128,512]{0,1:T(8,128)(2,1)}), bf16[1024,512]{0,1:T(8,128)(2,1)}) %all-gather.7.cloned.1.call-update) | async-done | bytes 1048592 | tf_op jit(solution)/shard_map/all_gather | solution.py:91
  51.6 40.3 %all-gather.5.cloned.1.call-done = bf16[1024,512]{0,1:T(8,128)(2,1)} async-done(((bf16[128,512]{0,1:T(8,128)(2,1)}), bf16[1024,512]{0,1:T(8,128)(2,1)}) %all-gather.5.cloned.1.call-update) | async-done | bytes 1048592 | tf_op jit(solution)/shard_map/all_gather | solution.py:92
  91.9 33.3 %while.16 = (s32[]{:T(128)}, f32[128,8,64]{0,2,1:T(8,128)S(1)}, f32[8,128]{1,0:T(8,128)S(1)}, bf16[1024,512]{0,1:T(8,128)(2,1)}, bf16[1024,512]{0,1:T(8,128)(2,1...) while((s32[]{:T(128)}, f32[128,8,64]{0,2,1:T(8,128)S(1)}, ...), condition=%wide.region_6.7_spmd.clone, body=%wide.region_2.6_spmd.clone.sunk | while | flops 219436672 | bytes 27240652 | solution.py:111
  93.4 3.0 %fusion.93 = (f32[8,128]{1,0:T(8,128)S(1)}, f32[8,128,512]{1,2,0:T(8,128)S(1)}, f32[8,512,128]{2,1,0:T(8,128)}) fusion(f32[8,512]{1,0:T(8,128)S(1)} %dynamic-slice_convert_fusion.2, pred[128,512]{0,1:T(8,128)(4,1)S(1)} %compare_and_fusion.2, bf16[512,8,64]{0,2,1:T(8,128)(2,1)S(1)} %bitcast.121, bf16[128,8,64]{0,2,1:T(8,128)(2,1)S(1)} %get-tuple-element.292), kind=kOutput, calls=%fused_computation.39.clone.1 | convolution fusion | flops 72875008 | bytes 4935680 | tf_op jit(solution)/shard_map/while/body/eval_jaxpr/qhd,khd->hqk/dot_general | solution.py:42
  96.4 5.0 %fusion.94 = f32[8,128,4,128]{1,0,3,2:T(8,128)S(1)} fusion(f32[8,128,4,128]{1,3,2,0:T(8,128)S(1)} %bitcast.119), kind=kOutput, calls=%fused_computation.23.clone.1 | output fusion | flops 66584576 | bytes 4194304 | tf_op jit(solution)/shard_map/reduce-window.6
  101.6 1.7 copy.38
  103.3 4.8 %fusion.97 = bf16[8,128,512]{1,2,0:T(8,128)(2,1)S(1)} fusion(f32[8,128,4,128]{1,3,2,0:T(8,128)} %copy.38, f32[8,512,128]{2,1,0:T(8,128)} %get-tuple-element.259, f32[8,128]{1,0:T(8,128)S(1)} %get-tuple-element.261, f32[8,512]{1,0:T(8,128)S(1)} %dynamic-slice_convert_fusion.2, pred[128,512]{0,1:T(8,128)(4,1)S(1)} %compare_and_fusion.2), kind=kLoop, calls=%fused_computation.12.clone.1 | loop fusion | flops 12058624 | bytes 5328896 | tf_op jit(solution)/shard_map/while/body/eval_jaxpr/convert_element_type | solution.py:55
  110.1 3.0 %fusion.93 = (f32[8,128]{1,0:T(8,128)S(1)}, f32[8,128,512]{1,2,0:T(8,128)S(1)}, f32[8,512,128]{2,1,0:T(8,128)}) fusion(f32[8,512]{1,0:T(8,128)S(1)} %dynamic-slice_convert_fusion.2, pred[128,512]{0,1:T(8,128)(4,1)S(1)} %compare_and_fusion.2, bf16[512,8,64]{0,2,1:T(8,128)(2,1)S(1)} %bitcast.121, bf16[128,8,64]{0,2,1:T(8,128)(2,1)S(1)} %get-tuple-element.292), kind=kOutput, calls=%fused_computation.39.clone.1 | convolution fusion | flops 72875008 | bytes 4935680 | tf_op jit(solution)/shard_map/while/body/eval_jaxpr/qhd,khd->hqk/dot_general | solution.py:42
  113.1 5.0 %fusion.94 = f32[8,128,4,128]{1,0,3,2:T(8,128)S(1)} fusion(f32[8,128,4,128]{1,3,2,0:T(8,128)S(1)} %bitcast.119), kind=kOutput, calls=%fused_computation.23.clone.1 | output fusion | flops 66584576 | bytes 4194304 | tf_op jit(solution)/shard_map/reduce-window.6
  118.3 1.7 copy.38
  120.0 4.8 %fusion.97 = bf16[8,128,512]{1,2,0:T(8,128)(2,1)S(1)} fusion(f32[8,128,4,128]{1,3,2,0:T(8,128)} %copy.38, f32[8,512,128]{2,1,0:T(8,128)} %get-tuple-element.259, f32[8,128]{1,0:T(8,128)S(1)} %get-tuple-element.261, f32[8,512]{1,0:T(8,128)S(1)} %dynamic-slice_convert_fusion.2, pred[128,512]{0,1:T(8,128)(4,1)S(1)} %compare_and_fusion.2), kind=kLoop, calls=%fused_computation.12.clone.1 | loop fusion | flops 12058624 | bytes 5328896 | tf_op jit(solution)/shard_map/while/body/eval_jaxpr/convert_element_type | solution.py:55
  125.2 2.9 %convolution_convert_fusion.1 = bf16[128,2048]{1,0:T(8,128)(2,1)} fusion(bf16[128,512]{0,1:T(8,128)(2,1)S(1)} %bitcast.123, bf16[512,2048]{1,0:T(8,128)(2,1)} %param.23), kind=kOutput, calls=%fused_computation.41 | convolution fusion | flops 268697600 | bytes 2752512 | tf_op jit(solution)/shard_map/dot_general | solution.py:113
  130.3 2.2 scatter_custom_fusion.1
  133.3 15.6 %reduce-scatter.3.cloned.1.call-done = bf16[128,512]{1,0:T(8,128)(2,1)} async-done(((bf16[128,2048]{1,0:T(8,128)(2,1)}), bf16[128,512]{1,0:T(8,128)(2,1)}) %reduce-scatter.3.cloned.1.call-update) | async-done | bytes 131088 | tf_op jit(solution)/shard_map/reduce_scatter | solution.py:133
  150.0 5.8 %psum.7 = f32[128]{0:T(128)S(1)} all-reduce(f32[128]{0:T(128)S(1)} %get-tuple-element.193), channel_id=1, replica_groups=mesh['sp'=8,'tp'=4] {'tp'}, use_global_device_ids=true, to_apply=%region_9.10 | all-reduce | flops 128 | bytes 1024 | tf_op jit(solution)/shard_map/psum | solution.py:140
  155.9 2.0 gather_fusion
  158.0 16.3 %all_to_all.10 = bf16[8,40,512]{2,1,0:T(8,128)(2,1)} all-to-all(bf16[8,40,512]{2,1,0:T(8,128)(2,1)S(1)} %broadcast_multiply_fusion), channel_id=1, replica_groups=mesh['sp'=8,'tp'=4] {'sp'}, dimensions={0} | all-to-all | bytes 655360 | tf_op jit(solution)/shard_map/all_to_all | solution.py:147
  174.6 15.6 %all-gather.9.cloned.1.call-done = bf16[8,40,2048]{2,1,0:T(8,128)(2,1)} async-done(((bf16[8,40,512]{2,1,0:T(8,128)(2,1)}), bf16[8,40,2048]{2,1,0:T(8,128)(2,1)}) %all-gather.9.cloned.1.call-update) | async-done | bytes 1310736 | tf_op jit(solution)/shard_map/all_gather | solution.py:146
  190.1 2.8 %fusion.33 = f32[8,40,512]{2,1,0:T(8,128)S(1)} fusion(bf16[8,40,2048]{2,1,0:T(8,128)(2,1)} %all-gather.9.cloned.1.call-done, bf16[1,2048,512]{2,1,0:T(8,128)(2,1)} %param.27), kind=kOutput, calls=%fused_computation.50 | convolution fusion | flops 671252480 | bytes 4063232 | tf_op jit(solution)/shard_map/scd,df->scf/dot_general | solution.py:152
  193.0 4.8 %convolution_convert_fusion = bf16[8,40,2048]{2,1,0:T(8,128)(2,1)} fusion(bf16[1,512,2048]{2,1,0:T(8,128)(2,1)S(1)} %copy-done, bf16[8,40,2048]{2,1,0:T(8,128)(2,1)} %all-gather.9.cloned.1.call-done, bf16[1,2048,512]{2,1,0:T(8,128)(2,1)} %param.28, f32[8,40,512]{2,1,0:T(8,128)S(1)} %fusion.33), kind=kOutput, calls=%fused_computation.40 | convolution fusion | flops 1344307200 | bytes 7471104 | tf_op jit(solution)/shard_map/scf,fd->scd/dot_general | solution.py:155
  197.8 26.6 %reduce-scatter.5.cloned.1.call-done = bf16[8,40,512]{2,1,0:T(8,128)(2,1)} async-done(((bf16[8,40,2048]{2,1,0:T(8,128)(2,1)}), bf16[8,40,512]{2,1,0:T(8,128)(2,1)}) %reduce-scatter.5.cloned.1.call-update) | async-done | bytes 327696 | tf_op jit(solution)/shard_map/reduce_scatter | solution.py:156
  224.4 5.5 %all-to-all-start.1 = ((bf16[8,40,512]{2,1,0:T(8,128)(2,1)}), bf16[8,40,512]{2,1,0:T(8,128)(2,1)S(1)}, u32[]{:S(2)}, u32[]{:S(2)}) async-start(bf16[8,40,512]{2,1,0:T(8,128)(2,1)} %reduce-scatter.5.cloned.1.call-done), calls=%async_computation.3 | async-start | bytes 655360 | tf_op jit(solution)/shard_map/all_to_all | solution.py:157
  230.0 10.0 %all-to-all-done.1 = bf16[8,40,512]{2,1,0:T(8,128)(2,1)S(1)} async-done(((bf16[8,40,512]{2,1,0:T(8,128)(2,1)}), bf16[8,40,512]{2,1,0:T(8,128)(2,1)S(1)}, u32[]{:S(2)}, u32[]{:S(2)}) %all-to-all-start.1) | async-done | bytes 327712 | tf_op jit(solution)/shard_map/all_to_all | solution.py:157
  (82 shorter events, 19.5 us)
Async XLA Ops:
  6.5 186.5 %copy-start = (bf16[1,512,2048]{2,1,0:T(8,128)(2,1)S(1)}, bf16[1,512,2048]{2,1,0:T(8,128)(2,1)}, u32[]{:S(2)}) copy-start(bf16[1,512,2048]{2,1,0:T(8,128)(2,1)} %param.29) | copy-start | bytes 6291460
  6.5 45.1 %all-gather.7.cloned.1.call-start = ((), (), s32[]{:S(2)}) async-start(), calls=%async_computation.5 | async-start | bytes 1179648 | tf_op jit(solution)/shard_map/all_gather | solution.py:91
  9.3 82.6 %all-gather.5.cloned.1.call-start = ((), (), s32[]{:S(2)}) async-start(), calls=%async_computation.4 | async-start | bytes 1179648 | tf_op jit(solution)/shard_map/all_gather | solution.py:92
  11.1 137.9 %reduce-scatter.3.cloned.1.call-start = ((), (), s32[]{:S(2)}) async-start(), calls=%async_computation.6 | async-start | bytes 655360 | tf_op jit(solution)/shard_map/reduce_scatter | solution.py:133
  125.1 3.4 %copy-start.1 = (s32[128,2]{0,1:T(2,128)S(1)}, s32[128,2]{0,1:T(2,128)}, u32[]{:S(2)}) copy-start(s32[128,2]{0,1:T(2,128)} %param.25) | copy-start | bytes 3076
  128.1 62.1 %all-gather.9.cloned.1.call-start = ((), (), s32[]{:S(2)}) async-start(), calls=%async_computation.7 | async-start | bytes 1638400 | tf_op jit(solution)/shard_map/all_gather | solution.py:146
  174.4 50.0 %reduce-scatter.5.cloned.1.call-start = ((), (), s32[]{:S(2)}) async-start(), calls=%async_computation.8 | async-start | bytes 1638400 | tf_op jit(solution)/shard_map/reduce_scatter | solution.py:156
  193.0 36.9 %copy-start.2 = (f32[128,2]{0,1:T(2,128)S(1)}, f32[128,2]{0,1:T(2,128)}, u32[]{:S(2)}) copy-start(f32[128,2]{0,1:T(2,128)} %param.26) | copy-start | bytes 3076
  224.4 15.7 %all-to-all-start.1 = ((bf16[8,40,512]{2,1,0:T(8,128)(2,1)}), bf16[8,40,512]{2,1,0:T(8,128)(2,1)S(1)}, u32[]{:S(2)}, u32[]{:S(2)}) async-start(bf16[8,40,512]{2,1,0:T(8,128)(2,1)} %reduce-scatter.5.cloned.1.call-done), calls=%async_computation.3 | async-start | bytes 655360 | tf_op jit(solution)/shard_map/all_to_all | solution.py:157
Sparse Core Ops, SparseCore 0:
  9.4 42.1 all-gather.6
  53.6 38.1 all-gather.4
  128.2 20.6 reduce-scatter.2
  174.5 15.6 all-gather.8
  197.9 26.4 reduce-scatter.4
